TPU v7x, 32 devices: a whole 2x2x4 slice. The times are simulated.
32 devices in a mesh: fs: 8 (over z, x), tp: 4 (over y, core).
Axes of the slice: x: 2, y: 2, z: 4, core: 2. Of those that a mesh axis runs over, the one named last changes fastest.
Arguments:
- tokens: bfloat16 [4096, 2048], P(('fs', 'tp')), may hold values from -6 to 6
- gate_weight: bfloat16 [2048, 6144], P('fs', 'tp'), may hold values from -0.125 to 0.125
- value_weight: bfloat16 [2048, 6144], P('fs', 'tp'), may hold values from -0.125 to 0.125
- gate_taps: float32 [3, 6144], P(None, 'tp'), may hold values from -3.5 to 3.5
- value_taps: float32 [3, 6144], P(None, 'tp'), may hold values from -3.5 to 3.5
- down_weight: bfloat16 [6144, 2048], P('tp', 'fs'), may hold values from -0.078125 to 0.078125
- norm_gain: float32 [2048], replicated, may hold values from 0.1 to 1.9
- norm_shift: float32 [2048], replicated, may hold values from -3 to 3
Outputs:
- mixed: bfloat16 [4096, 2048], P(('fs', 'tp'))
All inputs are finite; a program needn't handle non-finite values.
Results may differ from a plain program's by a relative error of at most 0.017.
Values may be sent and summed in bfloat16 or wider, within the bound.
A program may use at most 256 MiB of HBM per device.

v0:
```python
import jax
import jax.numpy as jnp
from jax import lax
from jax.sharding import PartitionSpec as P


def causal_mix(pre, kernel_taps):
    leading = jnp.zeros((2, pre.shape[1]), jnp.float32)
    padded = jnp.concatenate([leading, pre.astype(jnp.float32)], axis=0)
    length = pre.shape[0]
    return (
        kernel_taps[0] * padded[0:length]
        + kernel_taps[1] * padded[1 : length + 1]
        + kernel_taps[2] * padded[2 : length + 2]
    )


def local(
    tokens, gate_weight, value_weight, gate_taps, value_taps, down_weight, norm_gain, norm_shift
):
    sequence = lax.all_gather(tokens, "tp", axis=0, tiled=True)

    def add_rows(segment):
        return jnp.dot(sequence, segment, preferred_element_type=jnp.float32)

    gate_sum = add_rows(lax.all_gather(gate_weight, "fs", axis=0, tiled=True))
    value_sum = add_rows(lax.all_gather(value_weight, "fs", axis=0, tiled=True))
    gate_mix = causal_mix(gate_sum.astype(jnp.bfloat16), gate_taps)
    value_mix = causal_mix(value_sum.astype(jnp.bfloat16), value_taps)
    hidden = (jax.nn.gelu(gate_mix, approximate=False) * value_mix).astype(jnp.bfloat16)
    partial_terms = jnp.dot(
        hidden,
        lax.all_gather(down_weight, "fs", axis=1, tiled=True),
        preferred_element_type=jnp.float32,
    )
    summed = lax.psum_scatter(
        partial_terms.astype(jnp.bfloat16), "tp", scatter_dimension=0, tiled=True
    ).astype(jnp.float32)
    average = jnp.mean(summed, axis=1, keepdims=True)
    centered = summed - average
    variance = jnp.mean(centered * centered, axis=1, keepdims=True)
    normed = centered * lax.rsqrt(variance + 1e-05) * norm_gain + norm_shift
    return normed.astype(jnp.bfloat16)


def solution(mesh):
    in_specs = (
        P(("fs", "tp"), None),
        P("fs", "tp"),
        P("fs", "tp"),
        P(None, "tp"),
        P(None, "tp"),
        P("tp", "fs"),
        P(),
        P(),
    )
    out_specs = P(("fs", "tp"), None)
    return jax.shard_map(local, mesh=mesh, in_specs=in_specs, out_specs=out_specs, check_vma=False)
```

profile of v0, /device:TPU:0, one launch (start us, length us, event | category | flops | bytes accessed | tf_op | source)
XLA Modules:
  0.0 394.9 jit_solution(5087503630397722218)
XLA Ops:
  6.5 0.0 all-gather.5.cloned.1.call-start
  6.5 0.7 all-gather.5.cloned.1.call-update
  7.3 0.0 all-gather.7.cloned.1.call-start
  7.3 0.7 all-gather.7.cloned.1.call-update
  8.0 0.0 all-gather.9.cloned.1.call-start
  8.1 0.7 all-gather.9.cloned.1.call-update
  8.7 0.0 all-gather.11.cloned.1.call-start
  8.8 0.5 all-gather.11.cloned.1.call-update
  9.3 0.0 reduce-scatter.2.cloned.1.call-start
  9.4 1.0 slice_reduce_fusion.2
  10.3 23.9 %all-gather.5.cloned.1.call-done = bf16[512,2048]{1,0:T(8,128)(2,1)} async-done(((bf16[128,2048]{1,0:T(8,128)(2,1)}), bf16[512,2048]{1,0:T(8,128)(2,1)}) %all-gather.5.cloned.1.call-update) | async-done | bytes 2097168 | tf_op jit(solution)/shard_map/all_gather | solution.py:21
  34.2 0.0 copy-start.2
  34.2 100.9 %all-gather.7.cloned.1.call-done = bf16[2048,1536]{1,0:T(8,128)(2,1)} async-done(((bf16[256,1536]{1,0:T(8,128)(2,1)}), bf16[2048,1536]{1,0:T(8,128)(2,1)}) %all-gather.7.cloned.1.call-update) | async-done | bytes 6291472 | tf_op jit(solution)/shard_map/all_gather | solution.py:26
  135.1 8.5 %fusion.12 = f32[512,1536]{1,0:T(8,128)} fusion(bf16[512,2048]{1,0:T(8,128)(2,1)} %all-gather.5.cloned.1.call-done, bf16[2048,1536]{1,0:T(8,128)(2,1)} %all-gather.7.cloned.1.call-done), kind=kOutput, calls=%fused_computation.25 | convolution fusion | flops 3222798336 | bytes 11534336 | tf_op jit(solution)/shard_map/dot_general | solution.py:24
  143.6 90.6 %all-gather.9.cloned.1.call-done = bf16[2048,1536]{1,0:T(8,128)(2,1)} async-done(((bf16[256,1536]{1,0:T(8,128)(2,1)}), bf16[2048,1536]{1,0:T(8,128)(2,1)}) %all-gather.9.cloned.1.call-update) | async-done | bytes 6291472 | tf_op jit(solution)/shard_map/all_gather | solution.py:27
  234.2 0.0 copy-done.2
  234.2 7.9 %fusion.11 = f32[512,1536]{1,0:T(8,128)} fusion(bf16[512,2048]{1,0:T(8,128)(2,1)S(1)} %copy-done.2, bf16[2048,1536]{1,0:T(8,128)(2,1)} %all-gather.9.cloned.1.call-done), kind=kOutput, calls=%fused_computation.23 | convolution fusion | flops 3222798336 | bytes 11534336 | tf_op jit(solution)/shard_map/dot_general | solution.py:24
  242.1 91.7 %all-gather.11.cloned.1.call-done = bf16[1536,2048]{1,0:T(8,128)(2,1)} async-done(((bf16[1536,256]{1,0:T(8,128)(2,1)}), bf16[1536,2048]{1,0:T(8,128)(2,1)}) %all-gather.11.cloned.1.call-update) | async-done | bytes 6291472 | tf_op jit(solution)/shard_map/all_gather | solution.py:33
  333.8 20.2 %convolution_convert_fusion = bf16[512,2048]{1,0:T(8,128)(2,1)} fusion(bf16[1536,2048]{1,0:T(8,128)(2,1)} %all-gather.11.cloned.1.call-done, f32[512,1536]{1,0:T(8,128)} %fusion.11, f32[512,1536]{1,0:T(8,128)} %fusion.12, f32[1536]{0:T(1024)S(1)} %get-tuple-element.9, f32[1536]{0:T(1024)S(1)} %get-tuple-element.10, f32[1536]{0:T(1024)S(1)} %get-tuple-element.8, ...), kind=kOutput, calls=%fused_computation.21 | convolution fusion | flops 3282042880 | bytes 14716928 | tf_op jit(solution)/shard_map/dot_general | solution.py:31
  354.0 0.0 copy-start
  354.0 0.0 copy-start.1
  354.0 0.0 reduce-scatter.2.cloned.1.call-update
  354.1 29.5 %reduce-scatter.2.cloned.1.call-done = bf16[128,2048]{1,0:T(8,128)(2,1)} async-done(((bf16[512,2048]{1,0:T(8,128)(2,1)}), bf16[128,2048]{1,0:T(8,128)(2,1)}) %reduce-scatter.2.cloned.1.call-update) | async-done | bytes 524304 | tf_op jit(solution)/shard_map/reduce_scatter | solution.py:36
  383.6 1.2 convert_reduce_fusion
  384.8 1.3 fusion.16
  386.1 0.0 copy-done
  386.1 0.0 copy-done.1
  386.1 2.2 fusion.19
  (2 shorter events, 0.0 us)
Async XLA Ops:
  6.5 27.7 %all-gather.5.cloned.1.call-start = ((), (), s32[]{:S(2)}) async-start(), calls=%async_computation.1 | async-start | bytes 2621440 | tf_op jit(solution)/shard_map/all_gather | solution.py:21
  7.3 127.9 %all-gather.7.cloned.1.call-start = ((), (), s32[]{:S(2)}) async-start(), calls=%async_computation.2 | async-start | bytes 7077888 | tf_op jit(solution)/shard_map/all_gather | solution.py:26
  8.0 226.2 %all-gather.9.cloned.1.call-start = ((), (), s32[]{:S(2)}) async-start(), calls=%async_computation.3 | async-start | bytes 7077888 | tf_op jit(solution)/shard_map/all_gather | solution.py:27
  8.7 325.1 %all-gather.11.cloned.1.call-start = ((), (), s32[]{:S(2)}) async-start(), calls=%async_computation.4 | async-start | bytes 7077888 | tf_op jit(solution)/shard_map/all_gather | solution.py:33
  9.3 374.3 %reduce-scatter.2.cloned.1.call-start = ((), (), s32[]{:S(2)}) async-start(), calls=%async_computation.5 | async-start | bytes 2621440 | tf_op jit(solution)/shard_map/reduce_scatter | solution.py:36
  34.2 200.0 %copy-start.2 = (bf16[512,2048]{1,0:T(8,128)(2,1)S(1)}, bf16[512,2048]{1,0:T(8,128)(2,1)}, u32[]{:S(2)}) copy-start(bf16[512,2048]{1,0:T(8,128)(2,1)} %all-gather.5.cloned.1.call-done) | copy-start | bytes 6291460
  354.0 32.1 %copy-start = (f32[2048]{0:T(1024)S(1)}, f32[2048]{0:T(1024)}, u32[]{:S(2)}) copy-start(f32[2048]{0:T(1024)} %param.15) | copy-start | bytes 24580
  354.0 32.1 %copy-start.1 = (f32[2048]{0:T(1024)S(1)}, f32[2048]{0:T(1024)}, u32[]{:S(2)}) copy-start(f32[2048]{0:T(1024)} %param.14) | copy-start | bytes 24580
Sparse Core Ops, SparseCore 0:
  8.9 25.2 all-gather.4
  36.4 98.6 all-gather.6
  137.3 96.8 all-gather.8
  236.1 97.6 all-gather.10
  354.2 29.3 reduce-scatter.1
where the time goes:
time: 395 us
  waiting for transfers between devices  339 us (86%)
  matrix products  36.6 us (9%)
  between operations  13.2 us (3%)
  other arithmetic  4.78 us (1%)
    all_gather x1, waiting for transfers between devices, local(): gate_sum = add_rows(lax.all_gather(gate_weight, 'fs', axis=0, tiled=True))  101 us
    all_gather x1, waiting for transfers between devices, local(): lax.all_gather(down_weight, 'fs', axis=1, tiled=True)  91.7 us
    all_gather x1, waiting for transfers between devices, local(): value_sum = add_rows(lax.all_gather(value_weight, 'fs', axis=0, tiled=True))  90.6 us
    reduce_scatter x1, waiting for transfers between devices, local(): lax.psum_scatter(partial_terms.astype(jnp.bfloat16), 'tp', scatter_dimens...  29.5 us
    all_gather x1, waiting for transfers between devices, local(): sequence = lax.all_gather(tokens, 'tp', axis=0, tiled=True)  23.9 us
    dot_general x1, matrix products, local(): jnp.dot(hidden, lax.all_gather(down_weight, 'fs', axis=1, tiled=True), pr...  20.2 us
    dot_general x2, matrix products, add_rows(): return jnp.dot(sequence, segment, preferred_element_type=jnp.float32)  16.4 us
  transfers between devices with their start and end apart: 5, of which 5 were waited for; matrix products, arithmetic and copies ran while one was open for 4% of the time, Pallas kernels for 0%

commit v1 on v0

v1 whole, which is shorter than its diff:
```python
import functools

import jax
import jax.numpy as jnp
from jax import lax
from jax.experimental import pallas as pl
from jax.experimental.pallas import tpu as pltpu
from jax.sharding import PartitionSpec as P

MESH = pl.DeviceIdType.MESH
LEAD = 8


def kernel(
    dims,
    x_ref, g_ref, v_ref, gt_ref, vt_ref, d_ref, gain_ref, shift_ref,
    out_ref,
    tok, gw, vw, dw, pre_g, pre_v, part, rc, ry, zr,
    tok_r, tz_s, ty_s, tc_s, w_r, wz_s, wx_s, rc_r, rc_s, ry_r, ry_s, zc_r, zc_s,
):
    nz, nx, ny, nc = dims
    rows, width = x_ref.shape
    depth = g_ref.shape[0]
    units = gw.shape[1]
    cols = d_ref.shape[1]
    fs = lax.axis_index("fs")
    tp = lax.axis_index("tp")
    z, x = fs // nx, fs % nx
    y, c = tp // nc, tp % nc
    length = ny * nc * rows

    def at(zz=z, xx=x, yy=y, cc=c):
        return {"fs": zz * nx + xx, "tp": yy * nc + cc}

    z_others = [(z + i) % nz for i in range(1, nz)]
    x_others = [(x + i) % nx for i in range(1, nx)]
    y_others = [(y + i) % ny for i in range(1, ny)]
    c_others = [(c + i) % nc for i in range(1, nc)]

    barrier = pltpu.get_barrier_semaphore()
    partners = (
        [at(zz=i) for i in z_others]
        + [at(xx=i) for i in x_others]
        + [at(yy=i) for i in y_others]
        + [at(cc=i) for i in c_others]
    )
    for partner in partners:
        pl.semaphore_signal(barrier, inc=1, device_id=partner, device_id_type=MESH)
    pl.semaphore_wait(barrier, len(partners))

    def copy(src, dst, send, recv, device):
        return pltpu.make_async_remote_copy(
            src_ref=src, dst_ref=dst, send_sem=send, recv_sem=recv,
            device_id=device, device_id_type=MESH,
        )

    def slot(zz, t):
        return tok.at[zz, pl.ds(pl.multiple_of(t * rows, rows), rows)]

    def tok_copy(src, zz, t, send, device):
        return copy(src, slot(zz, t), send, tok_r.at[zz, t], device)

    def tok_z(src, zz, way):
        return tok_copy(src, zz, tp, tz_s.at[way, zz], at(zz=z + 1 - 2 * way))

    def tok_y(src, zz, yy):
        return tok_copy(src, zz, tp, ty_s.at[zz, yy], at(yy=yy))

    def tok_c(src, zz, yy, cc):
        return tok_copy(src, zz, yy * nc + c, tc_s.at[zz, yy, cc], at(cc=cc))

    def tok_wait(zz, t):
        tok_copy(slot(zz, t), zz, t, tz_s.at[0, 0], partners[0]).wait_recv()

    def spread(src, zz):
        for yy in y_others:
            tok_y(src, zz, yy).start()
        for cc in c_others:
            tok_c(src, zz, y, cc).start()

    def piece(kind, zz):
        if kind == 2:
            return d_ref.at[pl.ds(pl.multiple_of(zz * units, 128), units)]
        ref = g_ref if kind == 0 else v_ref
        return ref.at[:, pl.ds(pl.multiple_of(zz * units, 128), units)]

    def place(kind, src):
        if kind == 2:
            return dw.at[:, pl.ds(pl.multiple_of(src * cols, cols), cols)]
        ref = gw if kind == 0 else vw
        return ref.at[pl.ds(pl.multiple_of(src * depth, depth), depth)]

    def w_z(kind, zz):
        return copy(piece(kind, zz), place(kind, fs), wz_s.at[kind, zz], w_r.at[kind, fs], at(zz=zz))

    def w_x(kind, src, zz, xx):
        return copy(src, place(kind, zz * nx + x), wx_s.at[kind, zz, xx], w_r.at[kind, zz * nx + x], at(xx=xx))

    def w_wait(kind, src):
        copy(place(kind, src), place(kind, src), wz_s.at[kind, 0], w_r.at[kind, src], partners[0]).wait_recv()

    def w_own(kind):
        for xx in x_others:
            w_x(kind, piece(kind, z), z, xx).start()

    def w_send(kind):
        for zz in z_others:
            w_z(kind, zz).start()

    def w_forward(kind):
        for zz in z_others:
            w_wait(kind, zz * nx + x)
            for xx in x_others:
                w_x(kind, place(kind, zz * nx + x), zz, xx).start()

    def relay(step):
        for way in range(2):
            zz = z - step + 2 * step * way

            @pl.when((zz >= 0) & (zz < nz))
            def _():
                tok_wait(zz, tp)
                if step < nz - 1:
                    ahead = z + 1 - 2 * way

                    @pl.when((ahead >= 0) & (ahead < nz))
                    def _():
                        tok_z(slot(zz, tp), zz, way).start()
                spread(slot(zz, tp), zz)

    for way in range(2):
        ahead = z + 1 - 2 * way

        @pl.when((ahead >= 0) & (ahead < nz))
        def _():
            tok_z(x_ref, z, way).start()

    w_own(0)
    w_own(1)
    w_own(2)
    spread(x_ref, z)
    w_send(0)
    jobs = [lambda: w_send(1), lambda: w_forward(0), lambda: w_send(2), lambda: w_forward(1)]
    tok[z, pl.ds(pl.multiple_of(tp * rows, rows), rows)] = x_ref[...]
    mine = pl.ds(pl.multiple_of(fs * depth, depth), depth)
    part_units = pl.ds(pl.multiple_of(z * units, 128), units)
    gw[mine, :] = g_ref[:, part_units]
    vw[mine, :] = v_ref[:, part_units]
    dw[:, pl.ds(pl.multiple_of(fs * cols, cols), cols)] = d_ref[part_units, :]
    for step in range(1, nz):
        relay(step)
        for _ in range(2):
            if jobs:
                jobs.pop(0)()
    while jobs:
        jobs.pop(0)()
    for i in range(nz):
        zz = (z + i) % nz
        for yy in y_others:
            tok_wait(zz, yy * nc + c)
            for cc in c_others:
                tok_c(slot(zz, yy * nc + c), zz, yy, cc).start()
    w_forward(2)
    for kind in range(3):
        for xx in x_others:
            for i in range(nz):
                w_wait(kind, i * nx + xx)

    half = (2 * z) // nz if nz > 1 else 0
    near = z + half * (nz - 1 - 2 * z)

    def order(k):
        j = nz - 1 - k
        past = (j - near - 1 + nz) // nz
        f = past * j + (1 - past) * (near - j)
        return f + half * (nz - 1 - 2 * f)

    def block(zz, t):
        return part.at[zz, pl.ds(pl.multiple_of(t * rows, rows), rows)]

    def rc_copy(zz, yy, cc):
        return copy(block(zz, yy * nc + cc), rc.at[zz, yy], rc_s.at[zz, yy], rc_r.at[zz, yy], at(cc=cc))

    def ry_copy(zz, yy):
        return copy(block(zz, yy * nc + c), ry.at[zz, y], ry_s.at[zz, yy], ry_r.at[zz, y], at(yy=yy))

    def ry_wait(zz, yy):
        copy(block(zz, tp), ry.at[zz, yy], ry_s.at[zz, yy], ry_r.at[zz, yy], partners[0]).wait_recv()

    def zc_copy(way, zz):
        return copy(block(zz, tp), zr.at[way, zz], zc_s.at[way, zz], zc_r.at[way, zz], at(zz=z + 1 - 2 * way))

    def zc_wait(way, zz):
        copy(block(zz, tp), zr.at[way, zz], zc_s.at[way, zz], zc_r.at[way, zz], partners[0]).wait_recv()

    def mix(pre, w, taps, zz):
        raw = jnp.dot(tok[zz], w[...], preferred_element_type=jnp.float32)
        pre[pl.ds(LEAD, length), :] = raw.astype(jnp.bfloat16).astype(jnp.float32)
        return (
            taps[0:1, part_units] * pre[pl.ds(LEAD - 2, length), :]
            + taps[1:2, part_units] * pre[pl.ds(LEAD - 1, length), :]
            + taps[2:3, part_units] * pre[pl.ds(LEAD, length), :]
        )

    pre_g[0:LEAD, :] = jnp.zeros((LEAD, units), jnp.float32)
    pre_v[0:LEAD, :] = jnp.zeros((LEAD, units), jnp.float32)

    def f32(ref):
        return ref[...].astype(jnp.float32)

    def body(k, carry):
        @pl.when(k < nz)
        def _():
            zz = order(k)
            for yy in range(ny):
                for cc in c_others:
                    tok_wait(zz, yy * nc + cc)
            gate = mix(pre_g, gw, gt_ref, zz)
            value = mix(pre_v, vw, vt_ref, zz)
            act = 0.5 * gate * (1.0 + lax.erf(gate * (0.5**0.5)))
            hidden = (act * value).astype(jnp.bfloat16)
            part[zz] = jnp.dot(hidden, dw[...], preferred_element_type=jnp.float32).astype(jnp.bfloat16)
            for yy in range(ny):
                for cc in c_others:
                    rc_copy(zz, yy, cc).start()

        @pl.when((k >= 1) & (k < nz + 1))
        def _():
            zz = order(k - 1)
            for yy in y_others + [y]:
                if nc > 1:
                    rc_copy(zz, yy, c_others[0]).wait_recv()
                    mine = block(zz, yy * nc + c)
                    mine[...] = (f32(mine) + f32(rc.at[zz, yy])).astype(jnp.bfloat16)
            for yy in y_others:
                ry_copy(zz, yy).start()

        @pl.when(k >= 2)
        def _():
            zz = order(k - 2)
            mine = block(zz, tp)
            total = f32(mine)
            for yy in y_others:
                ry_wait(zz, yy)
                total = total + f32(ry.at[zz, yy])
            mine[...] = total.astype(jnp.bfloat16)
            t = k - 2
            for way in range(2):
                pos = z + way * (nz - 1 - 2 * z)
                far = nz - 1 - t + pos
                dest = far + way * (nz - 1 - 2 * far)

                @pl.when((t < nz - 1) & (t >= pos) & (pos < nz - 1))
                def _():
                    @pl.when(pos > 0)
                    def _():
                        zc_wait(way, dest)
                        sent = block(dest, tp)
                        sent[...] = (f32(sent) + f32(zr.at[way, dest])).astype(jnp.bfloat16)

                    zc_copy(way, dest).start()

        return carry

    lax.fori_loop(0, nz + 2, body, 0)

    for way in range(2):
        back = z - 1 + 2 * way

        @pl.when((back >= 0) & (back < nz))
        def _():
            zc_wait(way, z)

        @pl.when((back < 0) | (back >= nz))
        def _():
            zr[way, z] = jnp.zeros((rows, width), jnp.bfloat16)

    summed = f32(block(z, tp)) + f32(zr.at[0, z]) + f32(zr.at[1, z])
    average = jnp.mean(summed, axis=1, keepdims=True)
    centered = summed - average
    variance = jnp.mean(centered * centered, axis=1, keepdims=True)
    normed = centered * lax.rsqrt(variance + 1e-05) * gain_ref[...] + shift_ref[...]
    out_ref[...] = normed.astype(out_ref.dtype)

    for way in range(2):
        ahead = z + 1 - 2 * way

        @pl.when((ahead >= 0) & (ahead < nz))
        def _():
            for step in range(nz - 1):
                zz = z - step + 2 * step * way

                @pl.when((zz >= 0) & (zz < nz))
                def _():
                    tok_z(slot(zz, tp), zz, way).wait_send()

                dest = z + (step + 1) * (1 - 2 * way)

                @pl.when((dest >= 0) & (dest < nz))
                def _():
                    zc_copy(way, dest).wait_send()

    for zz in range(nz):
        for yy in y_others:
            tok_y(slot(zz, tp), zz, yy).wait_send()
            ry_copy(zz, yy).wait_send()
        for yy in range(ny):
            for cc in c_others:
                tok_c(slot(zz, yy * nc + c), zz, yy, cc).wait_send()
                rc_copy(zz, yy, cc).wait_send()
    for kind in range(3):
        for zz in z_others:
            w_z(kind, zz).wait_send()
        for zz in range(nz):
            for xx in x_others:
                w_x(kind, place(kind, zz * nx + x), zz, xx).wait_send()


def solution(mesh):
    n_fs, n_tp = mesh.shape["fs"], mesh.shape["tp"]
    nc = 2 if n_tp % 2 == 0 else 1
    ny = n_tp // nc

    def local(tokens, gate_weight, value_weight, gate_taps, value_taps, down_weight, gain, shift):
        rows, width = tokens.shape
        depth, held = gate_weight.shape
        nz = 4
        while nz > 1 and (n_fs % nz or held % (128 * nz)):
            nz //= 2
        nx = n_fs // nz
        units = held // nz
        length = n_tp * rows
        bf16 = jnp.bfloat16
        dma = pltpu.SemaphoreType.DMA
        return pl.pallas_call(
            functools.partial(kernel, (nz, nx, ny, nc)),
            out_shape=jax.ShapeDtypeStruct((rows, width), bf16),
            in_specs=[pl.BlockSpec(memory_space=pltpu.VMEM)] * 8,
            out_specs=pl.BlockSpec(memory_space=pltpu.VMEM),
            scratch_shapes=[
                pltpu.VMEM((nz, length, width), bf16),
                pltpu.VMEM((width, units), bf16),
                pltpu.VMEM((width, units), bf16),
                pltpu.VMEM((units, width), bf16),
                pltpu.VMEM((length + LEAD, units), jnp.float32),
                pltpu.VMEM((length + LEAD, units), jnp.float32),
                pltpu.VMEM((nz, length, width), bf16),
                pltpu.VMEM((nz, ny, rows, width), bf16),
                pltpu.VMEM((nz, ny, rows, width), bf16),
                pltpu.VMEM((2, nz, rows, width), bf16),
                dma((nz, n_tp)),
                dma((2, nz)),
                dma((nz, ny)),
                dma((nz, ny, nc)),
                dma((3, n_fs)),
                dma((3, nz)),
                dma((3, nz, nx)),
                dma((nz, ny)),
                dma((nz, ny)),
                dma((nz, ny)),
                dma((nz, ny)),
                dma((2, nz)),
                dma((2, nz)),
            ],
            compiler_params=pltpu.CompilerParams(
                collective_id=0, has_side_effects=True, vmem_limit_bytes=60 * 2**20
            ),
        )(
            tokens, gate_weight, value_weight, gate_taps, value_taps, down_weight,
            gain.reshape(1, width), shift.reshape(1, width),
        )

    in_specs = (
        P(("fs", "tp"), None),
        P("fs", "tp"),
        P("fs", "tp"),
        P(None, "tp"),
        P(None, "tp"),
        P("tp", "fs"),
        P(),
        P(),
    )
    out_specs = P(("fs", "tp"), None)
    return jax.shard_map(local, mesh=mesh, in_specs=in_specs, out_specs=out_specs, check_vma=False)
```

time: 395 us -> 168 us (0.43)
  waiting for transfers between devices: 339 us -> 0 us
  Pallas kernels: 0 us -> 166 us
  matrix products: 36.6 us -> 0 us
  between operations: 13.2 us -> 0.01 us
  other arithmetic: 4.78 us -> 0 us
    all_gather x4 -> x0, waiting for transfers between devices: 307 us -> none  [the longest x1 101 us: local(): gate_sum = add_rows(lax.all_gather(gate_weight, 'fs', axis=0, tiled=True))]
    pallas_call x0 -> x1, Pallas kernels: none -> 166 us  [local(): pl.pallas_call(functools.partial(kernel, (nz, nx, ny, nc)), out_shape=jax...]
    dot_general x3 -> x0, matrix products: 36.6 us -> none  [the longest x1 20.2 us: local(): jnp.dot(hidden, lax.all_gather(down_weight, 'fs', axis=1, tiled=True), pr...]
    reduce_scatter x1 -> x0, waiting for transfers between devices: 29.5 us -> none  [local(): lax.psum_scatter(partial_terms.astype(jnp.bfloat16), 'tp', scatter_dimens...]
  transfers between devices with their start and end apart: 5 -> 0, of which waited for: 5 -> 0; matrix products, arithmetic and copies ran while one was open for 4% -> 0% of each run, Pallas kernels for 0% -> 0%
where the time goes in v1:
time: 168 us
  Pallas kernels  166 us (99%)
  local copies, waits for them, and re-layouts  1.88 us (1%)
    pallas_call x1, Pallas kernels, local(): pl.pallas_call(functools.partial(kernel, (nz, nx, ny, nc)), out_shape=jax...  166 us

profile of v1, /device:TPU:0, one launch (start us, length us, event | category | flops | bytes accessed | tf_op | source)
XLA Modules:
  0.0 167.6 jit_solution(2731844990206951225)
XLA Ops:
  0.0 165.7 %shard_map.82 = bf16[128,2048]{1,0:T(8,128)(2,1)} custom-call(bf16[128,2048]{1,0:T(8,128)(2,1)} %x_ref.1, bf16[256,1536]{1,0:T(8,128)(2,1)} %g_ref.1, bf16[256,1536]{1,0:T(8,128)(2,1)} %v_ref.1, f32[3,1536]{1,0:T(4,128)} %gt_ref.1, f32[3,1536]{1,0:T(4,128)} %vt_ref.1, bf16[1536,256]{1,0:T(8,128)(2,1)} %d_ref.1, f32[1,2048]{1,0:T(1,128)} %bitcast.2, ...), custom_call_target="tpu_custom_call" | custom-call | tf_op jit(solution)/shard_map/pallas_call | solution.py:335
  165.8 1.9 %copy.10 = bf16[128,2048]{1,0:T(8,128)(2,1)} copy(bf16[128,2048]{1,0:T(8,128)(2,1)} %shard_map.82) | data formatting | bytes 1048576

commit v2 on v1

--- a/solution.py
+++ b/solution.py
@@ -15,7 +15,7 @@
     dims,
     x_ref, g_ref, v_ref, gt_ref, vt_ref, d_ref, gain_ref, shift_ref,
     out_ref,
-    tok, gw, vw, dw, pre_g, pre_v, part, rc, ry, zr,
+    tok, gw, vw, dw, pre_g, pre_v, hid, part, rc, ry, zr,
     tok_r, tz_s, ty_s, tc_s, w_r, wz_s, wx_s, rc_r, rc_s, ry_r, ry_s, zc_r, zc_s,
 ):
     nz, nx, ny, nc = dims
@@ -103,15 +103,25 @@
         for xx in x_others:
             w_x(kind, piece(kind, z), z, xx).start()
 
+    def both(step, act):
+        for way in range(2):
+            zz = z - step + 2 * step * way
+
+            @pl.when((zz >= 0) & (zz < nz))
+            def _():
+                act(zz)
+
     def w_send(kind):
-        for zz in z_others:
-            w_z(kind, zz).start()
-
-    def w_forward(kind):
-        for zz in z_others:
+        for step in range(1, nz):
+            both(step, lambda zz: w_z(kind, zz).start())
+
+    def w_forward(kind, step):
+        def act(zz):
             w_wait(kind, zz * nx + x)
             for xx in x_others:
                 w_x(kind, place(kind, zz * nx + x), zz, xx).start()
+
+        both(step, act)
 
     def relay(step):
         for way in range(2):
@@ -136,11 +146,8 @@
             tok_z(x_ref, z, way).start()
 
     w_own(0)
+    spread(x_ref, z)
     w_own(1)
-    w_own(2)
-    spread(x_ref, z)
-    w_send(0)
-    jobs = [lambda: w_send(1), lambda: w_forward(0), lambda: w_send(2), lambda: w_forward(1)]
     tok[z, pl.ds(pl.multiple_of(tp * rows, rows), rows)] = x_ref[...]
     mine = pl.ds(pl.multiple_of(fs * depth, depth), depth)
     part_units = pl.ds(pl.multiple_of(z * units, 128), units)
@@ -149,31 +156,36 @@
     dw[:, pl.ds(pl.multiple_of(fs * cols, cols), cols)] = d_ref[part_units, :]
     for step in range(1, nz):
         relay(step)
-        for _ in range(2):
-            if jobs:
-                jobs.pop(0)()
-    while jobs:
-        jobs.pop(0)()
-    for i in range(nz):
-        zz = (z + i) % nz
+        if step == min(2, nz - 1):
+            for kind in range(3):
+                w_send(kind)
+            w_own(2)
+    for kind in range(2):
+        for step in range(1, nz):
+            w_forward(kind, step)
+
+    half = (2 * z) // nz if nz > 1 else 0
+    near = z + half * (nz - 1 - 2 * z)
+
+    def order(j):
+        past = (j - near - 1 + nz) // nz
+        f = past * j + (1 - past) * (near - j)
+        return f + half * (nz - 1 - 2 * f)
+
+    def far_order(k):
+        return order(nz - 1 - k)
+
+    def cross(zz):
         for yy in y_others:
             tok_wait(zz, yy * nc + c)
             for cc in c_others:
                 tok_c(slot(zz, yy * nc + c), zz, yy, cc).start()
-    w_forward(2)
-    for kind in range(3):
+
+    cross(order(0))
+    for kind in range(2):
         for xx in x_others:
             for i in range(nz):
                 w_wait(kind, i * nx + xx)
-
-    half = (2 * z) // nz if nz > 1 else 0
-    near = z + half * (nz - 1 - 2 * z)
-
-    def order(k):
-        j = nz - 1 - k
-        past = (j - near - 1 + nz) // nz
-        f = past * j + (1 - past) * (near - j)
-        return f + half * (nz - 1 - 2 * f)
 
     def block(zz, t):
         return part.at[zz, pl.ds(pl.multiple_of(t * rows, rows), rows)]
@@ -208,25 +220,35 @@
     def f32(ref):
         return ref[...].astype(jnp.float32)
 
+    for k in range(nz):
+        zz = order(k)
+        if k + 1 < nz:
+            cross(order(k + 1))
+        for yy in range(ny):
+            for cc in c_others:
+                tok_wait(zz, yy * nc + cc)
+        gate = mix(pre_g, gw, gt_ref, zz)
+        value = mix(pre_v, vw, vt_ref, zz)
+        act = 0.5 * gate * (1.0 + lax.erf(gate * (0.5**0.5)))
+        hid[zz] = (act * value).astype(jnp.bfloat16)
+        if k + 1 < nz:
+            w_forward(2, k + 1)
+    for xx in x_others:
+        for i in range(nz):
+            w_wait(2, i * nx + xx)
+
     def body(k, carry):
         @pl.when(k < nz)
         def _():
-            zz = order(k)
-            for yy in range(ny):
-                for cc in c_others:
-                    tok_wait(zz, yy * nc + cc)
-            gate = mix(pre_g, gw, gt_ref, zz)
-            value = mix(pre_v, vw, vt_ref, zz)
-            act = 0.5 * gate * (1.0 + lax.erf(gate * (0.5**0.5)))
-            hidden = (act * value).astype(jnp.bfloat16)
-            part[zz] = jnp.dot(hidden, dw[...], preferred_element_type=jnp.float32).astype(jnp.bfloat16)
+            zz = far_order(k)
+            part[zz] = jnp.dot(hid[zz], dw[...], preferred_element_type=jnp.float32).astype(jnp.bfloat16)
             for yy in range(ny):
                 for cc in c_others:
                     rc_copy(zz, yy, cc).start()
 
         @pl.when((k >= 1) & (k < nz + 1))
         def _():
-            zz = order(k - 1)
+            zz = far_order(k - 1)
             for yy in y_others + [y]:
                 if nc > 1:
                     rc_copy(zz, yy, c_others[0]).wait_recv()
@@ -237,7 +259,7 @@
 
         @pl.when(k >= 2)
         def _():
-            zz = order(k - 2)
+            zz = far_order(k - 2)
             mine = block(zz, tp)
             total = f32(mine)
             for yy in y_others:
@@ -344,6 +366,7 @@
                 pltpu.VMEM((units, width), bf16),
                 pltpu.VMEM((length + LEAD, units), jnp.float32),
                 pltpu.VMEM((length + LEAD, units), jnp.float32),
+                pltpu.VMEM((nz, length, units), bf16),
                 pltpu.VMEM((nz, length, width), bf16),
                 pltpu.VMEM((nz, ny, rows, width), bf16),
                 pltpu.VMEM((nz, ny, rows, width), bf16),

time: 168 us -> 162 us (0.964)
  Pallas kernels: 166 us -> 160 us
    pallas_call x1, Pallas kernels: 166 us -> 160 us  [local(): pl.pallas_call(functools.partial(kernel, (nz, nx, ny, nc)), out_shape=jax...]
where the time goes in v2:
time: 162 us
  Pallas kernels  160 us (99%)
  local copies, waits for them, and re-layouts  1.88 us (1%)
    pallas_call x1, Pallas kernels, local(): pl.pallas_call(functools.partial(kernel, (nz, nx, ny, nc)), out_shape=jax...  160 us

profile of v2, /device:TPU:0, one launch (start us, length us, event | category | flops | bytes accessed | tf_op | source)
XLA Modules:
  0.0 162.0 jit_solution(9667789392697180486)
XLA Ops:
  0.0 160.1 %shard_map.82 = bf16[128,2048]{1,0:T(8,128)(2,1)} custom-call(bf16[128,2048]{1,0:T(8,128)(2,1)} %x_ref.1, bf16[256,1536]{1,0:T(8,128)(2,1)} %g_ref.1, bf16[256,1536]{1,0:T(8,128)(2,1)} %v_ref.1, f32[3,1536]{1,0:T(4,128)} %gt_ref.1, f32[3,1536]{1,0:T(4,128)} %vt_ref.1, bf16[1536,256]{1,0:T(8,128)(2,1)} %d_ref.1, f32[1,2048]{1,0:T(1,128)} %bitcast.2, ...), custom_call_target="tpu_custom_call" | custom-call | tf_op jit(solution)/shard_map/pallas_call | solution.py:357
  160.1 1.9 %copy.10 = bf16[128,2048]{1,0:T(8,128)(2,1)} copy(bf16[128,2048]{1,0:T(8,128)(2,1)} %shard_map.82) | data formatting | bytes 1048576
